TPU v7x, 512 devices: a 8x2x16 block of a 8x16x16 slice. The times are simulated.
512 devices in a mesh: grp: 2 (over y), ep: 16 (over z), tp: 16 (over x, core).
Axes of the slice: x: 8, y: 2, z: 16, core: 2. Of those that a mesh axis runs over, the one named last changes fastest.
The devices are a block of a 8x16x16 slice.
Arguments:
- tokens: bfloat16 [192, 2048], P('grp', 'ep'), parts along dimension 0, may hold values from -70 to 70
- first_gain: float32 [2048], replicated, may hold values from 0.1 to 1.9
- w_query: bfloat16 [2048, 2048], P('ep', 'tp'), may hold values from -0.125 to 0.125
- w_key: bfloat16 [2048, 2048], P('ep', 'tp'), may hold values from -0.125 to 0.125
- w_value: bfloat16 [2048, 4096], P('ep', 'tp'), may hold values from -0.125 to 0.125
- w_outgate: bfloat16 [2048, 4096], P('ep', 'tp'), may hold values from -0.125 to 0.125
- w_input: bfloat16 [2048, 16], replicated, may hold values from -0.125 to 0.125
- w_forget: bfloat16 [2048, 16], replicated, may hold values from -0.125 to 0.125
- input_bias: float32 [16], replicated, may hold values from -3 to 3
- forget_bias: float32 [16], replicated, may hold values from -2 to 5
- head_gain: float32 [4096], replicated, may hold values from 0.1 to 1.9
- w_project: bfloat16 [4096, 2048], P('tp', 'ep'), may hold values from -0.09375 to 0.09375
- cell_state: float32 [192, 16, 128, 256], P(('grp', 'ep'), 'tp'), parts along dimension 0, may hold values from -6 to 6
- norm_state: float32 [192, 16, 128], P(('grp', 'ep'), 'tp'), parts along dimension 0, may hold values from -6 to 6
- max_state: float32 [192, 16], P(('grp', 'ep'), 'tp'), parts along dimension 0, may hold values from -110 to 110
- second_gain: float32 [2048], replicated, may hold values from 0.1 to 1.9
- routes: int32 [192, 2], P('grp'), parts along dimension 0, may hold values from 0 to 15, all different within a row; in each aligned block of 6 rows (0 to 5, 6 to 11, ...) at most 2 rows name the same one
- route_weight: float32 [192, 2], P('grp'), parts along dimension 0, may hold values from 0.2 to 1
- expert_gate: bfloat16 [16, 2048, 4096], P('ep', None, 'tp'), may hold values from -0.125 to 0.125
- expert_up: bfloat16 [16, 2048, 4096], P('ep', None, 'tp'), may hold values from -0.125 to 0.125
- expert_down: bfloat16 [16, 4096, 2048], P('ep', 'tp'), may hold values from -0.09375 to 0.09375
Outputs:
- layer_out: bfloat16 [192, 2048], P('grp', 'ep'), parts along dimension 0
- new_cell: float32 [192, 16, 128, 256], P(('grp', 'ep'), 'tp'), parts along dimension 0
- new_norm: float32 [192, 16, 128], P(('grp', 'ep'), 'tp'), parts along dimension 0
- new_max: float32 [192, 16], P(('grp', 'ep'), 'tp'), parts along dimension 0
There are 2 independent parts, one for each index of `grp`. A program takes and returns all parts, laid end to end along the dimension named above; an argument that names none is the same for every part. Nothing has to cross between parts.
Inputs may be any that keep to these rules, and one draw needn't show every extreme that they name: `routes`: each sequence names 2 different experts. In each aligned block of 6 sequences no expert is named by more than 2 of them, a bound that some block reaches.
All inputs are finite; a program needn't handle non-finite values.
Results may differ from a plain program's by a relative error of at most 0.0065.
Values may be sent and summed in bfloat16 or wider, within the bound.
No kernel may reach another device: no remote copies, remote signals or barrier semaphores. Data moves between devices by JAX's collectives and lax.ppermute only.
A program may use at most 64 MiB of HBM per device.

v0:
```python
import jax
import jax.numpy as jnp
from jax import lax
from jax.sharding import PartitionSpec as P

EXP_DEV = 1
NORM_EPS = 1e-05
HEAD_EPS = 1e-06


def from_everyone(array, axis):
    peers = lax.axis_size(axis)
    return lax.all_to_all(
        jnp.broadcast_to(array[None], (peers, *array.shape)), axis, 0, 0, tiled=True
    )


def taken_together(array, axis):
    everything = from_everyone(array, axis)
    return jnp.sum(everything, axis=0)


def in_one(arrays, axis):
    ends = [0]
    for a in arrays:
        ends.append(ends[-1] + a.size)
    subtotal = taken_together(jnp.concatenate([a.ravel() for a in arrays]), axis)
    return tuple((subtotal[b:e].reshape(a.shape) for a, b, e in zip(arrays, ends, ends[1:])))


def cut_along(array, dim, peers):
    lengths = array.shape
    blocks = array.reshape(*lengths[:dim], peers, lengths[dim] // peers, *lengths[dim + 1 :])
    return jnp.moveaxis(blocks, dim, 0)


def summed_on_arrival(array, axis, dim):
    blocks = cut_along(array, dim, lax.axis_size(axis))
    arrived = lax.all_to_all(blocks, axis, split_axis=0, concat_axis=0, tiled=True)
    return arrived.astype(jnp.float32).sum(axis=0)


def summed_on_arrival_2(array, axis, dim):
    blocks = cut_along(array, dim, lax.axis_size(axis))
    arrived = lax.all_to_all(blocks, axis, split_axis=0, concat_axis=0, tiled=True)
    return arrived.sum(axis=0)


def side_by_side(arrays, axis, dim, along):
    ends, at = ([], 0)
    for a in arrays[:-1]:
        at += a.shape[along]
        ends.append(at)
    both = jnp.concatenate(arrays, axis=along)
    return tuple(jnp.split(summed_on_arrival_2(both, axis, dim), ends, axis=along))


def joined_along(blocks, dim):
    lengths = list(blocks.shape[1:])
    lengths[dim] *= blocks.shape[0]
    return jnp.moveaxis(blocks, 0, dim).reshape(lengths)


def gather_directly(array, axis, dim):
    return joined_along(from_everyone(array, axis), dim)


def gathered_total(array, axis):
    blocks = lax.all_gather(array, axis)
    return blocks.sum(axis=0)


def row_norm(stream_rows, gain_whole):
    col_count = stream_rows.shape[1]
    gain_cols = lax.dynamic_slice_in_dim(gain_whole, lax.axis_index("ep") * col_count, col_count, 0)
    values = stream_rows.astype(jnp.float32)
    totals, squares = in_one((jnp.sum(values, axis=1), jnp.sum(values * values, axis=1)), "ep")
    features = col_count * lax.axis_size("ep")
    row_mean = totals / features
    spread = squares / features - row_mean * row_mean
    inv_scale = lax.rsqrt(spread + NORM_EPS)
    return ((values - row_mean[:, None]) * inv_scale[:, None] * gain_cols).astype(jnp.bfloat16)


def expert_act(gate_sum, up_sum):
    return (jax.nn.silu(gate_sum) * up_sum).astype(jnp.bfloat16)


def scatter_slots(active, expert_down):
    slot_major = jnp.moveaxis(active, 1, 0)
    return summed_on_arrival(
        jnp.einsum(
            "pef,efd->ped", slot_major, expert_down, preferred_element_type=jnp.float32
        ).astype(jnp.bfloat16),
        "tp",
        0,
    ).astype(jnp.bfloat16)


def on_device(
    tokens,
    first_gain,
    w_query,
    w_key,
    w_value,
    w_outgate,
    w_input,
    w_forget,
    input_bias,
    forget_bias,
    head_gain,
    w_project,
    cell_state,
    norm_state,
    max_state,
    second_gain,
    routes,
    route_weight,
    expert_gate,
    expert_up,
    expert_down,
):
    blocks = lax.axis_size("ep")
    columns = tokens.shape[1]
    seq_total = tokens.shape[0]
    seq_local = seq_total // blocks
    heads_local = cell_state.shape[1]
    key_size = cell_state.shape[2]
    value_size = cell_state.shape[3]
    col_start = lax.axis_index("ep") * columns
    head_start = lax.axis_index("tp") * heads_local
    normed = row_norm(tokens, first_gain)
    input_cols = lax.dynamic_slice(w_input, (col_start, head_start), (columns, heads_local))
    forget_cols = lax.dynamic_slice(w_forget, (col_start, head_start), (columns, heads_local))

    def project_part(weight):
        return jnp.dot(normed, weight, preferred_element_type=jnp.float32)

    summed = side_by_side(
        (
            project_part(w_query),
            project_part(w_key),
            project_part(w_value),
            project_part(w_outgate),
            project_part(input_cols),
            project_part(forget_cols),
        ),
        "ep",
        0,
        1,
    )
    queries = summed[0].astype(jnp.bfloat16).reshape(seq_local, heads_local, key_size)
    key_rows = summed[1].astype(jnp.bfloat16).reshape(seq_local, heads_local, key_size)
    value_rows = summed[2].astype(jnp.bfloat16).reshape(seq_local, heads_local, value_size)
    outgate = summed[3].astype(jnp.bfloat16)
    input_pre = summed[4] + lax.dynamic_slice_in_dim(input_bias, head_start, heads_local, 0)
    forget_pre = summed[5] + lax.dynamic_slice_in_dim(forget_bias, head_start, heads_local, 0)
    carried = jax.nn.log_sigmoid(forget_pre) + max_state
    new_max = jnp.maximum(carried, input_pre)
    keep_old = jnp.exp(carried - new_max)
    admit_new = jnp.exp(input_pre - new_max)
    key_float = key_rows.astype(jnp.float32)
    value_float = value_rows.astype(jnp.float32)
    new_cell = (
        keep_old[:, :, None, None] * cell_state
        + admit_new[:, :, None, None] * key_float[:, :, :, None] * value_float[:, :, None, :]
    )
    new_norm = keep_old[:, :, None] * norm_state + admit_new[:, :, None] * key_float
    query_float = queries.astype(jnp.float32) * key_size ** (-0.5)
    readout = jnp.einsum("shk,shkv->shv", query_float, new_cell, precision=lax.Precision.HIGHEST)
    head_mean = jnp.mean(readout, axis=2, keepdims=True)
    centred = readout - head_mean
    head_var = jnp.mean(centred * centred, axis=2, keepdims=True)
    gains_here = lax.dynamic_slice_in_dim(
        head_gain, head_start * value_size, heads_local * value_size, 0
    )
    mixed_heads = (
        (centred * lax.rsqrt(head_var + HEAD_EPS)).reshape(seq_local, heads_local * value_size)
        * gains_here
        * jax.nn.sigmoid(outgate.astype(jnp.float32))
    ).astype(jnp.bfloat16)
    head_terms = jnp.dot(
        gather_directly(mixed_heads, "ep", 0), w_project, preferred_element_type=jnp.float32
    )
    mixer_out = gathered_total(head_terms, "tp")
    stream = (tokens.astype(jnp.float32) + mixer_out).astype(jnp.bfloat16)
    second_normed = row_norm(stream, second_gain)
    experts = blocks * EXP_DEV
    top_count = routes.shape[1]
    capacity = max(2, 2 * seq_local * top_count // experts)
    slot_count = blocks * capacity
    expert_ids = lax.broadcasted_iota(jnp.int32, (1, 1, experts), 2)
    matches = routes[:, :, None] == expert_ids
    routed = jnp.sum(matches.astype(jnp.int32), axis=1)
    combine = jnp.sum(jnp.where(matches, route_weight[:, :, None], 0.0), axis=1)
    running = (
        jnp.cumsum(routed.reshape(blocks, seq_local, experts), axis=1).reshape(seq_total, experts)
        - routed
    )
    block_ids = lax.broadcasted_iota(jnp.int32, (seq_total, experts), 0) // seq_local
    slot_of = block_ids * capacity + running
    slot_ids = lax.broadcasted_iota(jnp.int32, (experts, slot_count, seq_total), 1)
    placed = (slot_of.T[:, None, :] == slot_ids) & (routed.T[:, None, :] > 0)
    picker = placed.astype(jnp.bfloat16)
    weighted = jnp.where(placed, combine.T[:, None, :], 0.0)
    outbound = jnp.einsum(
        "eps,sd->epd", picker, second_normed, preferred_element_type=jnp.float32
    ).astype(jnp.bfloat16)
    arrived = lax.all_to_all(outbound, "ep", split_axis=0, concat_axis=2, tiled=True)
    gate_sum = jnp.einsum("end,edf->enf", arrived, expert_gate, preferred_element_type=jnp.float32)
    up_sum = jnp.einsum("end,edf->enf", arrived, expert_up, preferred_element_type=jnp.float32)
    active = expert_act(gate_sum, up_sum)
    share = scatter_slots(active, expert_down)
    back = lax.all_to_all(share, "ep", split_axis=2, concat_axis=1, tiled=True)
    every_slot = gather_directly(back, "tp", 0)
    moe_out = jnp.einsum(
        "eps,ped->sd", weighted, every_slot.astype(jnp.float32), precision=lax.Precision.HIGHEST
    )
    layer_out = (stream.astype(jnp.float32) + moe_out).astype(jnp.bfloat16)
    return (layer_out, new_cell, new_norm, new_max)


def solution(mesh):
    placed = (
        P("grp", "ep"),
        P(),
        P("ep", "tp"),
        P("ep", "tp"),
        P("ep", "tp"),
        P("ep", "tp"),
        P(),
        P(),
        P(),
        P(),
        P(),
        P("tp", "ep"),
        P(("grp", "ep"), "tp", None, None),
        P(("grp", "ep"), "tp", None),
        P(("grp", "ep"), "tp"),
        P(),
        P("grp", None),
        P("grp", None),
        P("ep", None, "tp"),
        P("ep", None, "tp"),
        P("ep", "tp", None),
    )
    return jax.shard_map(
        on_device,
        mesh=mesh,
        in_specs=placed,
        out_specs=(
            P("grp", "ep"),
            P(("grp", "ep"), "tp", None, None),
            P(("grp", "ep"), "tp", None),
            P(("grp", "ep"), "tp"),
        ),
        check_vma=False,
    )
```

profile of v0, /device:TPU:65, one launch (start us, length us, event | category | flops | bytes accessed | tf_op | source)
XLA Modules:
  0.0 232.7 jit_solution(2197950431508416456)
XLA Ops:
  0.6 0.9 convert_reduce_fusion.1
  2.3 44.2 %all-to-all-start = ((f32[16,1,192]{2,1,0:T(1,128)}), f32[16,1,192]{2,1,0:T(1,128)S(1)}, u32[]{:S(2)}, u32[]{:S(2)}) async-start(f32[16,1,192]{2,1,0:T(1,128)} %broadcast_in_dim.26), calls=%async_computation | async-start | bytes 32768 | tf_op jit(solution)/shard_map/all_to_all | solution.py:13
  47.3 10.4 %all-to-all-done = f32[16,1,192]{2,1,0:T(1,128)S(1)} async-done(((f32[16,1,192]{2,1,0:T(1,128)}), f32[16,1,192]{2,1,0:T(1,128)S(1)}, u32[]{:S(2)}, u32[]{:S(2)}) %all-to-all-start) | async-done | bytes 12320 | tf_op jit(solution)/shard_map/all_to_all | solution.py:13
  57.9 0.9 fusion.46
  58.9 0.9 fusion.48
  62.6 0.8 copy-done.7
  63.6 0.9 concatenate.23
  64.5 4.1 %all-to-all-start.1 = ((f32[16,6,770]{2,1,0:T(8,128)}), f32[16,6,770]{2,1,0:T(8,128)S(1)}, u32[]{:S(2)}, u32[]{:S(2)}) async-start(f32[16,6,770]{2,1,0:T(8,128)} %concatenate.23), calls=%async_computation.1 | async-start | bytes 917504 | tf_op jit(solution)/shard_map/all_to_all | solution.py:45
  72.3 17.0 %all-to-all-done.1 = f32[16,6,770]{2,1,0:T(8,128)S(1)} async-done(((f32[16,6,770]{2,1,0:T(8,128)}), f32[16,6,770]{2,1,0:T(8,128)S(1)}, u32[]{:S(2)}, u32[]{:S(2)}) %all-to-all-start.1) | async-done | bytes 295712 | tf_op jit(solution)/shard_map/all_to_all | solution.py:45
  89.3 1.5 exponential_reduce_fusion.1
  92.7 11.5 %all-to-all-start.2 = ((bf16[16,6,256]{2,1,0:T(8,128)(2,1)}), bf16[16,6,256]{2,1,0:T(8,128)(2,1)S(1)}, u32[]{:S(2)}, u32[]{:S(2)}) async-start(bf16[16,6,256]{2,1,0:T(8,128)(2,1)} %broadcast_in_dim.27), calls=%async_computation.2 | async-start | bytes 131072 | tf_op jit(solution)/shard_map/all_to_all | solution.py:13
  104.2 11.4 %all-to-all-done.2 = bf16[16,6,256]{2,1,0:T(8,128)(2,1)S(1)} async-done(((bf16[16,6,256]{2,1,0:T(8,128)(2,1)}), bf16[16,6,256]{2,1,0:T(8,128)(2,1)S(1)}, u32[]{:S(2)}, u32[]{:S(2)}) %all-to-all-start.2) | async-done | bytes 49184 | tf_op jit(solution)/shard_map/all_to_all | solution.py:13
  115.7 22.3 %all-gather = f32[1536,128]{1,0:T(8,128)S(1)} all-gather(f32[96,128]{1,0:T(8,128)S(1)} %fusion.74), channel_id=2, replica_groups=mesh['grp'=2,'ep'=16,'tp'=16] {'tp'}, dimensions={0}, use_global_device_ids=true | all-gather | bytes 835584 | tf_op jit(solution)/shard_map/all_gather | solution.py:69
  139.0 3.9 %all-to-all-start.3 = ((f32[16,1,192]{2,1,0:T(1,128)}), f32[16,1,192]{2,1,0:T(1,128)S(1)}, u32[]{:S(2)}, u32[]{:S(2)}) async-start(f32[16,1,192]{2,1,0:T(1,128)} %broadcast_in_dim.32), calls=%async_computation.3 | async-start | bytes 32768 | tf_op jit(solution)/shard_map/all_to_all | solution.py:13
  143.7 10.2 %all-to-all-done.3 = f32[16,1,192]{2,1,0:T(1,128)S(1)} async-done(((f32[16,1,192]{2,1,0:T(1,128)}), f32[16,1,192]{2,1,0:T(1,128)S(1)}, u32[]{:S(2)}, u32[]{:S(2)}) %all-to-all-start.3) | async-done | bytes 12320 | tf_op jit(solution)/shard_map/all_to_all | solution.py:13
  154.3 14.6 %all_to_all.56 = bf16[16,32,128]{2,1,0:T(8,128)(2,1)S(1)} all-to-all(bf16[16,32,128]{2,1,0:T(8,128)(2,1)S(1)} %convolution_convert_fusion.1), channel_id=1, replica_groups=mesh['grp'=2,'ep'=16,'tp'=16] {'ep'}, dimensions={0} | all-to-all | bytes 262144 | tf_op jit(solution)/shard_map/all_to_all | solution.py:209
  170.1 16.3 %all_to_all.57 = bf16[16,2,1,2048]{3,1,2,0:T(2,128)(2,1)S(1)} all-to-all(bf16[16,2,1,2048]{3,1,2,0:T(2,128)(2,1)S(1)} %bitcast.105), channel_id=1, replica_groups=mesh['grp'=2,'ep'=16,'tp'=16] {'tp'}, dimensions={0} | all-to-all | bytes 262144 | tf_op jit(solution)/shard_map/all_to_all | solution.py:39
  186.5 0.9 copy.101
  187.9 11.5 %reduce.12 = bf16[2048,2]{1,0:T(8,128)(2,1)S(1)} reduce(bf16[2048,1,2]{2,1,0:T(2,128)(2,1)S(1)} %bitcast.99, bf16[]{:T(256)} %broadcast.140), dimensions={1}, to_apply=%bitcast.86.reduce_sub_computation | reduce | bytes 16386
  200.1 15.1 %all_to_all.58 = bf16[16,2,128]{2,1,0:T(2,128)(2,1)S(1)} all-to-all(bf16[16,2,128]{2,1,0:T(2,128)(2,1)S(1)} %reshape.218), channel_id=1, replica_groups=mesh['grp'=2,'ep'=16,'tp'=16] {'ep'}, dimensions={0} | all-to-all | bytes 16384 | tf_op jit(solution)/shard_map/all_to_all | solution.py:214
  215.1 1.2 reshape.219
  217.7 4.7 %all-to-all-start.7 = ((bf16[16,2,16,128]{3,1,2,0:T(2,128)(2,1)}), bf16[16,2,16,128]{3,1,2,0:T(2,128)(2,1)S(1)}, u32[]{:S(2)}, u32[]{:S(2)}) async-start(bf16[16,2,16,128]{3,1,2,0:T(2,128)(2,1)} %broadcast_in_dim.34), calls=%async_computation.7 | async-start | bytes 262144 | tf_op jit(solution)/shard_map/all_to_all | solution.py:13
  223.7 7.9 %all-to-all-done.7 = bf16[16,2,16,128]{3,1,2,0:T(2,128)(2,1)S(1)} async-done(((bf16[16,2,16,128]{3,1,2,0:T(2,128)(2,1)}), bf16[16,2,16,128]{3,1,2,0:T(2,128)(2,1)S(1)}, u32[]{:S(2)}, u32[]{:S(2)}) %all-to-all-start.7) | async-done | bytes 131104 | tf_op jit(solution)/shard_map/all_to_all | solution.py:13
  231.7 1.0 fusion.2
  (102 shorter events, 17.7 us)
Async XLA Ops:
  0.6 168.6 %copy-start = (bf16[1,256,2048]{2,1,0:T(8,128)(2,1)S(1)}, bf16[1,256,2048]{2,1,0:T(8,128)(2,1)}, u32[]{:S(2)}) copy-start(bf16[1,256,2048]{2,1,0:T(8,128)(2,1)} %param.41) | copy-start | bytes 3145732
  2.3 55.4 %all-to-all-start = ((f32[16,1,192]{2,1,0:T(1,128)}), f32[16,1,192]{2,1,0:T(1,128)S(1)}, u32[]{:S(2)}, u32[]{:S(2)}) async-start(f32[16,1,192]{2,1,0:T(1,128)} %broadcast_in_dim.26), calls=%async_computation | async-start | bytes 32768 | tf_op jit(solution)/shard_map/all_to_all | solution.py:13
  46.5 11.3 %copy-start.5 = (bf16[96,128]{1,0:T(8,128)(2,1)S(1)}, bf16[96,128]{1,0:T(8,128)(2,1)}, u32[]{:S(2)}) copy-start(bf16[96,128]{1,0:T(8,128)(2,1)} %param.21) | copy-start | bytes 73732
  59.8 0.8 copy-start.9
  60.7 0.8 copy-start.10
  61.6 0.8 copy-start.6
  62.6 0.9 copy-start.7
  64.5 26.5 %copy-start.4 = (f32[6,1,128,256]{3,2,1,0:T(8,128)S(1)}, f32[6,1,128,256]{3,2,1,0:T(8,128)}, u32[]{:S(2)}) copy-start(f32[6,1,128,256]{3,2,1,0:T(8,128)} %param.33) | copy-start | bytes 2359300
  64.5 24.8 %all-to-all-start.1 = ((f32[16,6,770]{2,1,0:T(8,128)}), f32[16,6,770]{2,1,0:T(8,128)S(1)}, u32[]{:S(2)}, u32[]{:S(2)}) async-start(f32[16,6,770]{2,1,0:T(8,128)} %concatenate.23), calls=%async_computation.1 | async-start | bytes 917504 | tf_op jit(solution)/shard_map/all_to_all | solution.py:45
  68.6 0.7 copy-start.15
  69.3 0.7 copy-start.16
  69.9 0.7 copy-start.14
  70.6 0.7 copy-start.11
  91.1 46.9 %copy-start.1 = (f32[6,1,128,256]{3,2,1,0:T(8,128)}, f32[6,1,128,256]{3,2,1,0:T(8,128)S(1)}, u32[]{:S(2)}) copy-start(f32[6,1,128,256]{3,2,1,0:T(8,128)S(1)} %multiply_add_fusion) | copy-start | bytes 2359300
  92.7 22.9 %all-to-all-start.2 = ((bf16[16,6,256]{2,1,0:T(8,128)(2,1)}), bf16[16,6,256]{2,1,0:T(8,128)(2,1)S(1)}, u32[]{:S(2)}, u32[]{:S(2)}) async-start(bf16[16,6,256]{2,1,0:T(8,128)(2,1)} %broadcast_in_dim.27), calls=%async_computation.2 | async-start | bytes 131072 | tf_op jit(solution)/shard_map/all_to_all | solution.py:13
  104.2 11.4 %copy-start.8 = (bf16[256,128]{1,0:T(8,128)(2,1)S(1)}, bf16[256,128]{1,0:T(8,128)(2,1)}, u32[]{:S(2)}) copy-start(bf16[256,128]{1,0:T(8,128)(2,1)} %param.32) | copy-start | bytes 196612
  138.1 30.8 %copy-start.3 = (bf16[1,2048,256]{2,1,0:T(8,128)(2,1)S(1)}, bf16[1,2048,256]{2,1,0:T(8,128)(2,1)}, u32[]{:S(2)}) copy-start(bf16[1,2048,256]{2,1,0:T(8,128)(2,1)} %param.39) | copy-start | bytes 3145732
  138.2 31.0 %copy-start.2 = (bf16[1,2048,256]{2,1,0:T(8,128)(2,1)S(1)}, bf16[1,2048,256]{2,1,0:T(8,128)(2,1)}, u32[]{:S(2)}) copy-start(bf16[1,2048,256]{2,1,0:T(8,128)(2,1)} %param.40) | copy-start | bytes 3145732
  139.0 14.9 %all-to-all-start.3 = ((f32[16,1,192]{2,1,0:T(1,128)}), f32[16,1,192]{2,1,0:T(1,128)S(1)}, u32[]{:S(2)}, u32[]{:S(2)}) async-start(f32[16,1,192]{2,1,0:T(1,128)} %broadcast_in_dim.32), calls=%async_computation.3 | async-start | bytes 32768 | tf_op jit(solution)/shard_map/all_to_all | solution.py:13
  217.7 4.7 %copy-start.13 = (f32[96,2]{0,1:T(2,128)S(1)}, f32[96,2]{0,1:T(2,128)}, u32[]{:S(2)}) copy-start(f32[96,2]{0,1:T(2,128)} %param.38) | copy-start | bytes 2308
  217.7 13.9 %all-to-all-start.7 = ((bf16[16,2,16,128]{3,1,2,0:T(2,128)(2,1)}), bf16[16,2,16,128]{3,1,2,0:T(2,128)(2,1)S(1)}, u32[]{:S(2)}, u32[]{:S(2)}) async-start(bf16[16,2,16,128]{3,1,2,0:T(2,128)(2,1)} %broadcast_in_dim.34), calls=%async_computation.7 | async-start | bytes 262144 | tf_op jit(solution)/shard_map/all_to_all | solution.py:13
  222.4 0.7 copy-start.12
where the time goes:
time: 234 us; the launch traced here: 233 us
  starting transfers between devices  68.5 us (29%)
  blocking collectives  68.3 us (29%)
  waiting for transfers between devices  56.8 us (24%)
  local copies, waits for them, and re-layouts  17.4 us (7%)
  other arithmetic  15.6 us (7%)
  matrix products  5.14 us (2%)
    all_to_all x4, starting transfers between devices, from_everyone(): lax.all_to_all(jnp.broadcast_to(array[None], (peers, *array.shape)), axis...  64.3 us
    all_to_all x4, waiting for transfers between devices, from_everyone(): lax.all_to_all(jnp.broadcast_to(array[None], (peers, *array.shape)), axis...  39.9 us
    all_gather x1, blocking collectives, gathered_total(): blocks = lax.all_gather(array, axis)  22.3 us
    all_to_all x1, waiting for transfers between devices, summed_on_arrival_2(): lax.all_to_all(blocks, axis, split_axis=0, concat_axis=0, tiled=True)  17 us
    all_to_all x1, blocking collectives, summed_on_arrival(): lax.all_to_all(blocks, axis, split_axis=0, concat_axis=0, tiled=True)  16.3 us
    all_to_all x1, blocking collectives, on_device(): back = lax.all_to_all(share, 'ep', split_axis=2, concat_axis=1, tiled=True)  15.1 us
    all_to_all x1, blocking collectives, on_device(): lax.all_to_all(outbound, 'ep', split_axis=0, concat_axis=2, tiled=True)  14.6 us
    unnamed x1, other arithmetic  11.5 us
  transfers between devices with their start and end apart: 5, of which 5 were waited for; matrix products, arithmetic and copies ran while one was open for 2% of the time, Pallas kernels for 0%

commit v1 on v0

--- a/solution.py
+++ b/solution.py
@@ -206,7 +206,10 @@
     outbound = jnp.einsum(
         "eps,sd->epd", picker, second_normed, preferred_element_type=jnp.float32
     ).astype(jnp.bfloat16)
-    arrived = lax.all_to_all(outbound, "ep", split_axis=0, concat_axis=2, tiled=True)
+    arrived = jnp.concatenate(
+        lax.all_to_all(jnp.stack(jnp.split(outbound, lax.axis_size("ep"), axis=0)), "ep", 0, 0),
+        axis=2,
+    )
     gate_sum = jnp.einsum("end,edf->enf", arrived, expert_gate, preferred_element_type=jnp.float32)
     up_sum = jnp.einsum("end,edf->enf", arrived, expert_up, preferred_element_type=jnp.float32)
     active = expert_act(gate_sum, up_sum)

time: 234 us -> 234 us (level)
    unnamed x40 -> x55, local copies, waits for them, and re-layouts: 7.97 us -> 8.09 us
where the time goes in v1:
time: 234 us; the launch traced here: 233 us
  starting transfers between devices  68.5 us (29%)
  blocking collectives  68.4 us (29%)
  waiting for transfers between devices  56.8 us (24%)
  local copies, waits for them, and re-layouts  17.5 us (7%)
  other arithmetic  15.6 us (7%)
  matrix products  5.14 us (2%)
    all_to_all x4, starting transfers between devices, from_everyone(): lax.all_to_all(jnp.broadcast_to(array[None], (peers, *array.shape)), axis...  64.3 us
    all_to_all x4, waiting for transfers between devices, from_everyone(): lax.all_to_all(jnp.broadcast_to(array[None], (peers, *array.shape)), axis...  39.9 us
    all_gather x1, blocking collectives, gathered_total(): blocks = lax.all_gather(array, axis)  22.3 us
    all_to_all x1, waiting for transfers between devices, summed_on_arrival_2(): lax.all_to_all(blocks, axis, split_axis=0, concat_axis=0, tiled=True)  17 us
    all_to_all x1, blocking collectives, summed_on_arrival(): lax.all_to_all(blocks, axis, split_axis=0, concat_axis=0, tiled=True)  16.3 us
    all_to_all x1, blocking collectives, on_device(): back = lax.all_to_all(share, 'ep', split_axis=2, concat_axis=1, tiled=True)  15.1 us
    all_to_all x1, blocking collectives, on_device(): lax.all_to_all(jnp.stack(jnp.split(outbound, lax.axis_size('ep'), axis=0)...  14.7 us
    unnamed x1, other arithmetic  11.5 us
  transfers between devices with their start and end apart: 5, of which 5 were waited for; matrix products, arithmetic and copies ran while one was open for 2% of the time, Pallas kernels for 0%

profile of v1, /device:TPU:65, one launch (start us, length us, event | category | flops | bytes accessed | tf_op | source)
XLA Modules:
  0.0 233.0 jit_solution(11145311257155469580)
XLA Ops:
  0.6 0.9 convert_reduce_fusion.1
  2.3 44.2 %all-to-all-start = ((f32[16,1,192]{2,1,0:T(1,128)}), f32[16,1,192]{2,1,0:T(1,128)S(1)}, u32[]{:S(2)}, u32[]{:S(2)}) async-start(f32[16,1,192]{2,1,0:T(1,128)} %broadcast_in_dim.26), calls=%async_computation | async-start | bytes 32768 | tf_op jit(solution)/shard_map/all_to_all | solution.py:13
  47.3 10.4 %all-to-all-done = f32[16,1,192]{2,1,0:T(1,128)S(1)} async-done(((f32[16,1,192]{2,1,0:T(1,128)}), f32[16,1,192]{2,1,0:T(1,128)S(1)}, u32[]{:S(2)}, u32[]{:S(2)}) %all-to-all-start) | async-done | bytes 12320 | tf_op jit(solution)/shard_map/all_to_all | solution.py:13
  57.9 0.9 fusion.46
  58.9 0.9 fusion.48
  62.6 0.8 copy-done.7
  63.6 0.9 concatenate.23
  64.5 4.1 %all-to-all-start.1 = ((f32[16,6,770]{2,1,0:T(8,128)}), f32[16,6,770]{2,1,0:T(8,128)S(1)}, u32[]{:S(2)}, u32[]{:S(2)}) async-start(f32[16,6,770]{2,1,0:T(8,128)} %concatenate.23), calls=%async_computation.1 | async-start | bytes 917504 | tf_op jit(solution)/shard_map/all_to_all | solution.py:45
  72.3 17.0 %all-to-all-done.1 = f32[16,6,770]{2,1,0:T(8,128)S(1)} async-done(((f32[16,6,770]{2,1,0:T(8,128)}), f32[16,6,770]{2,1,0:T(8,128)S(1)}, u32[]{:S(2)}, u32[]{:S(2)}) %all-to-all-start.1) | async-done | bytes 295712 | tf_op jit(solution)/shard_map/all_to_all | solution.py:45
  89.3 1.5 exponential_reduce_fusion.1
  92.7 11.5 %all-to-all-start.2 = ((bf16[16,6,256]{2,1,0:T(8,128)(2,1)}), bf16[16,6,256]{2,1,0:T(8,128)(2,1)S(1)}, u32[]{:S(2)}, u32[]{:S(2)}) async-start(bf16[16,6,256]{2,1,0:T(8,128)(2,1)} %broadcast_in_dim.27), calls=%async_computation.2 | async-start | bytes 131072 | tf_op jit(solution)/shard_map/all_to_all | solution.py:13
  104.2 11.4 %all-to-all-done.2 = bf16[16,6,256]{2,1,0:T(8,128)(2,1)S(1)} async-done(((bf16[16,6,256]{2,1,0:T(8,128)(2,1)}), bf16[16,6,256]{2,1,0:T(8,128)(2,1)S(1)}, u32[]{:S(2)}, u32[]{:S(2)}) %all-to-all-start.2) | async-done | bytes 49184 | tf_op jit(solution)/shard_map/all_to_all | solution.py:13
  115.7 22.3 %all-gather = f32[1536,128]{1,0:T(8,128)S(1)} all-gather(f32[96,128]{1,0:T(8,128)S(1)} %fusion.74), channel_id=2, replica_groups=mesh['grp'=2,'ep'=16,'tp'=16] {'tp'}, dimensions={0}, use_global_device_ids=true | all-gather | bytes 835584 | tf_op jit(solution)/shard_map/all_gather | solution.py:69
  138.9 3.9 %all-to-all-start.3 = ((f32[16,1,192]{2,1,0:T(1,128)}), f32[16,1,192]{2,1,0:T(1,128)S(1)}, u32[]{:S(2)}, u32[]{:S(2)}) async-start(f32[16,1,192]{2,1,0:T(1,128)} %broadcast_in_dim.32), calls=%async_computation.3 | async-start | bytes 32768 | tf_op jit(solution)/shard_map/all_to_all | solution.py:13
  143.7 10.2 %all-to-all-done.3 = f32[16,1,192]{2,1,0:T(1,128)S(1)} async-done(((f32[16,1,192]{2,1,0:T(1,128)}), f32[16,1,192]{2,1,0:T(1,128)S(1)}, u32[]{:S(2)}, u32[]{:S(2)}) %all-to-all-start.3) | async-done | bytes 12320 | tf_op jit(solution)/shard_map/all_to_all | solution.py:13
  154.5 14.7 %all_to_all.46 = bf16[16,1,32,128]{3,2,1,0:T(8,128)(2,1)S(1)} all-to-all(bf16[16,1,32,128]{3,2,1,0:T(8,128)(2,1)S(1)} %constant_dynamic-update-slice_fusion), channel_id=1, replica_groups=mesh['grp'=2,'ep'=16,'tp'=16] {'ep'}, dimensions={0} | all-to-all | bytes 262144 | tf_op jit(solution)/shard_map/all_to_all | solution.py:210
  170.4 16.3 %all_to_all.47 = bf16[16,2,1,2048]{3,1,2,0:T(2,128)(2,1)S(1)} all-to-all(bf16[16,2,1,2048]{3,1,2,0:T(2,128)(2,1)S(1)} %bitcast.167), channel_id=1, replica_groups=mesh['grp'=2,'ep'=16,'tp'=16] {'tp'}, dimensions={0} | all-to-all | bytes 262144 | tf_op jit(solution)/shard_map/all_to_all | solution.py:39
  186.8 0.9 copy.101
  188.2 11.5 %reduce.12 = bf16[2048,2]{1,0:T(8,128)(2,1)S(1)} reduce(bf16[2048,1,2]{2,1,0:T(2,128)(2,1)S(1)} %bitcast.161, bf16[]{:T(256)} %broadcast.140), dimensions={1}, to_apply=%bitcast.148.reduce_sub_computation | reduce | bytes 16386
  200.4 15.1 %all_to_all.48 = bf16[16,2,128]{2,1,0:T(2,128)(2,1)S(1)} all-to-all(bf16[16,2,128]{2,1,0:T(2,128)(2,1)S(1)} %reshape.223), channel_id=1, replica_groups=mesh['grp'=2,'ep'=16,'tp'=16] {'ep'}, dimensions={0} | all-to-all | bytes 16384 | tf_op jit(solution)/shard_map/all_to_all | solution.py:217
  215.5 1.2 reshape.224
  218.0 4.7 %all-to-all-start.7 = ((bf16[16,2,16,128]{3,1,2,0:T(2,128)(2,1)}), bf16[16,2,16,128]{3,1,2,0:T(2,128)(2,1)S(1)}, u32[]{:S(2)}, u32[]{:S(2)}) async-start(bf16[16,2,16,128]{3,1,2,0:T(2,128)(2,1)} %broadcast_in_dim.34), calls=%async_computation.7 | async-start | bytes 262144 | tf_op jit(solution)/shard_map/all_to_all | solution.py:13
  224.1 7.9 %all-to-all-done.7 = bf16[16,2,16,128]{3,1,2,0:T(2,128)(2,1)S(1)} async-done(((bf16[16,2,16,128]{3,1,2,0:T(2,128)(2,1)}), bf16[16,2,16,128]{3,1,2,0:T(2,128)(2,1)S(1)}, u32[]{:S(2)}, u32[]{:S(2)}) %all-to-all-start.7) | async-done | bytes 131104 | tf_op jit(solution)/shard_map/all_to_all | solution.py:13
  232.1 1.0 fusion.2
  (118 shorter events, 17.8 us)
Async XLA Ops:
  0.6 168.9 %copy-start = (bf16[1,256,2048]{2,1,0:T(8,128)(2,1)S(1)}, bf16[1,256,2048]{2,1,0:T(8,128)(2,1)}, u32[]{:S(2)}) copy-start(bf16[1,256,2048]{2,1,0:T(8,128)(2,1)} %param.41) | copy-start | bytes 3145732
  2.3 55.4 %all-to-all-start = ((f32[16,1,192]{2,1,0:T(1,128)}), f32[16,1,192]{2,1,0:T(1,128)S(1)}, u32[]{:S(2)}, u32[]{:S(2)}) async-start(f32[16,1,192]{2,1,0:T(1,128)} %broadcast_in_dim.26), calls=%async_computation | async-start | bytes 32768 | tf_op jit(solution)/shard_map/all_to_all | solution.py:13
  46.5 11.3 %copy-start.5 = (bf16[96,128]{1,0:T(8,128)(2,1)S(1)}, bf16[96,128]{1,0:T(8,128)(2,1)}, u32[]{:S(2)}) copy-start(bf16[96,128]{1,0:T(8,128)(2,1)} %param.21) | copy-start | bytes 73732
  59.8 0.8 copy-start.9
  60.7 0.8 copy-start.10
  61.6 0.8 copy-start.6
  62.6 0.9 copy-start.7
  64.5 26.5 %copy-start.4 = (f32[6,1,128,256]{3,2,1,0:T(8,128)S(1)}, f32[6,1,128,256]{3,2,1,0:T(8,128)}, u32[]{:S(2)}) copy-start(f32[6,1,128,256]{3,2,1,0:T(8,128)} %param.33) | copy-start | bytes 2359300
  64.5 24.8 %all-to-all-start.1 = ((f32[16,6,770]{2,1,0:T(8,128)}), f32[16,6,770]{2,1,0:T(8,128)S(1)}, u32[]{:S(2)}, u32[]{:S(2)}) async-start(f32[16,6,770]{2,1,0:T(8,128)} %concatenate.23), calls=%async_computation.1 | async-start | bytes 917504 | tf_op jit(solution)/shard_map/all_to_all | solution.py:45
  68.6 0.7 copy-start.15
  69.3 0.7 copy-start.16
  69.9 0.7 copy-start.14
  70.6 0.7 copy-start.11
  91.1 46.9 %copy-start.1 = (f32[6,1,128,256]{3,2,1,0:T(8,128)}, f32[6,1,128,256]{3,2,1,0:T(8,128)S(1)}, u32[]{:S(2)}) copy-start(f32[6,1,128,256]{3,2,1,0:T(8,128)S(1)} %multiply_add_fusion) | copy-start | bytes 2359300
  92.7 22.9 %all-to-all-start.2 = ((bf16[16,6,256]{2,1,0:T(8,128)(2,1)}), bf16[16,6,256]{2,1,0:T(8,128)(2,1)S(1)}, u32[]{:S(2)}, u32[]{:S(2)}) async-start(bf16[16,6,256]{2,1,0:T(8,128)(2,1)} %broadcast_in_dim.27), calls=%async_computation.2 | async-start | bytes 131072 | tf_op jit(solution)/shard_map/all_to_all | solution.py:13
  104.2 11.4 %copy-start.8 = (bf16[256,128]{1,0:T(8,128)(2,1)S(1)}, bf16[256,128]{1,0:T(8,128)(2,1)}, u32[]{:S(2)}) copy-start(bf16[256,128]{1,0:T(8,128)(2,1)} %param.32) | copy-start | bytes 196612
  138.1 31.2 %copy-start.3 = (bf16[1,2048,256]{2,1,0:T(8,128)(2,1)S(1)}, bf16[1,2048,256]{2,1,0:T(8,128)(2,1)}, u32[]{:S(2)}) copy-start(bf16[1,2048,256]{2,1,0:T(8,128)(2,1)} %param.39) | copy-start | bytes 3145732
  138.9 14.9 %all-to-all-start.3 = ((f32[16,1,192]{2,1,0:T(1,128)}), f32[16,1,192]{2,1,0:T(1,128)S(1)}, u32[]{:S(2)}, u32[]{:S(2)}) async-start(f32[16,1,192]{2,1,0:T(1,128)} %broadcast_in_dim.32), calls=%async_computation.3 | async-start | bytes 32768 | tf_op jit(solution)/shard_map/all_to_all | solution.py:13
  154.2 15.3 %copy-start.2 = (bf16[1,2048,256]{2,1,0:T(8,128)(2,1)S(1)}, bf16[1,2048,256]{2,1,0:T(8,128)(2,1)}, u32[]{:S(2)}) copy-start(bf16[1,2048,256]{2,1,0:T(8,128)(2,1)} %param.40) | copy-start | bytes 3145732
  218.0 4.7 %copy-start.13 = (f32[96,2]{0,1:T(2,128)S(1)}, f32[96,2]{0,1:T(2,128)}, u32[]{:S(2)}) copy-start(f32[96,2]{0,1:T(2,128)} %param.38) | copy-start | bytes 2308
  218.0 13.9 %all-to-all-start.7 = ((bf16[16,2,16,128]{3,1,2,0:T(2,128)(2,1)}), bf16[16,2,16,128]{3,1,2,0:T(2,128)(2,1)S(1)}, u32[]{:S(2)}, u32[]{:S(2)}) async-start(bf16[16,2,16,128]{3,1,2,0:T(2,128)(2,1)} %broadcast_in_dim.34), calls=%async_computation.7 | async-start | bytes 262144 | tf_op jit(solution)/shard_map/all_to_all | solution.py:13
  222.7 0.7 copy-start.12
